TPU v7x, 256 devices: a 4x2x16 block of a 4x16x16 slice. The times are simulated.
256 devices in a mesh: grp: 2 (over y), ep: 32 (over z, core), tp: 4 (over x).
Axes of the slice: x: 4, y: 2, z: 16, core: 2. Of those that a mesh axis runs over, the one named last changes fastest.
The devices are a block of a 4x16x16 slice.
Arguments:
- query_plain: bfloat16 [16384, 512], P(('grp', 'ep'), 'tp'), parts along dimension 0, may hold values from -400 to 400
- query_rotary: bfloat16 [16384, 256], P(('grp', 'ep'), 'tp'), parts along dimension 0, may hold values from -6 to 6
- latent_input: bfloat16 [16384, 256], P(('grp', 'ep')), parts along dimension 0, may hold values from -6 to 6
- rotary_key: bfloat16 [16384, 32], P(('grp', 'ep')), parts along dimension 0, may hold values from -6 to 6
- key_weight: bfloat16 [256, 512], P(None, 'tp'), may hold values from -0.375 to 0.375
- value_weight: bfloat16 [256, 512], P(None, 'tp'), may hold values from -0.375 to 0.375
- latent_gain: bfloat16 [256], replicated, may hold values from 0.099609375 to 1.8984375
- head_gain: bfloat16 [512], P('tp'), may hold values from 0.099609375 to 1.8984375
- out_weight: bfloat16 [512, 2048], P('tp'), may hold values from -0.25 to 0.25
- expert_input: bfloat16 [32768, 2048], P(('grp', 'ep', 'tp')), parts along dimension 0, may hold values from -6 to 6
- expert_gain: bfloat16 [2048], replicated, may hold values from 0.099609375 to 1.8984375
- routes: int32 [32768, 2], P(('grp', 'ep', 'tp')), parts along dimension 0, may hold values from 0 to 31, all different within a row; in each aligned block of 128 rows (0 to 127, 128 to 255, ...) at most 9 rows name the same one
- route_weight: float32 [32768, 2], P(('grp', 'ep', 'tp')), parts along dimension 0, may hold values from 0.1 to 1
- gate_weight: bfloat16 [32, 2048, 3584], P('ep', None, 'tp'), may hold values from -0.125 to 0.125
- up_weight: bfloat16 [32, 2048, 3584], P('ep', None, 'tp'), may hold values from -0.125 to 0.125
- down_weight: bfloat16 [32, 3584, 2048], P('ep', 'tp'), may hold values from -0.09375 to 0.09375
Outputs:
- attended: bfloat16 [16384, 2048], P(('grp', 'ep', 'tp')), parts along dimension 0
- expert_out: bfloat16 [32768, 2048], P(('grp', 'ep', 'tp')), parts along dimension 0
There are 2 independent parts, one for each index of `grp`. A program takes and returns all parts, laid end to end along the dimension named above; an argument that names none is the same for every part. Nothing has to cross between parts.
Inputs may be any that keep to these rules, and one draw needn't show every extreme that they name: `routes`: each of the 128 rows of one device names 2 different experts; no expert is named by more than 9 rows of one device, a bound that some block reaches of some device.
All inputs are finite; a program needn't handle non-finite values.
Results may differ from a plain program's by a relative error of at most 0.012.
Values may be sent and summed in bfloat16 or wider, within the bound.
No kernel may reach another device: no remote copies, remote signals or barrier semaphores. Data moves between devices by JAX's collectives and lax.ppermute only.
A program may use at most 128 MiB of HBM per device.

v0:
```python
import jax
import jax.numpy as jnp
from jax import lax
from jax.sharding import Mesh
from jax.sharding import PartitionSpec as P

PLAIN_DIM = 64
ROTARY_DIM = 32
VALUE_DIM = 64
TOP = 2
EP = ("ep_0", "ep_1")
GRP_EP = ("grp", "ep_0", "ep_1")
GRP_EP_TP = ("grp", "ep_0", "ep_1", "tp")
EPSILON = 1e-06
THETA = 10000.0
key_span = 2048


def sent_together(arrays, axis, dim, along):
    ends, at = ([], 0)
    for a in arrays[:-1]:
        at += a.shape[along]
        ends.append(at)
    both = jnp.concatenate(arrays, axis=along)
    return tuple(jnp.split(lax.all_gather(both, axis, axis=dim, tiled=True), ends, axis=along))


def in_blocks(array, dim, size):
    lengths = array.shape
    tiles = array.reshape(*lengths[:dim], size, lengths[dim] // size, *lengths[dim + 1 :])
    return jnp.moveaxis(tiles, dim, 0)


def sum_at_owner(array, axis, dim):
    size = lax.axis_size(axis)
    tiles = lax.all_to_all(in_blocks(array, dim, size), axis, 0, 0, tiled=True)
    return jnp.sum(tiles.astype(jnp.float32), axis=0)


def joined_along(tiles, dim):
    tiles = jnp.moveaxis(tiles, 0, dim)
    lengths = tiles.shape
    return tiles.reshape(*lengths[:dim], lengths[dim] * lengths[dim + 1], *lengths[dim + 2 :])


def moved_by_axis(tiles, axes, sequence):
    lengths = [lax.axis_size(a) for a in axes]
    tiles = tiles.reshape(*lengths, *tiles.shape[1:])
    for k in sequence:
        tiles = lax.all_to_all(tiles, axes[k], split_axis=k, concat_axis=k, tiled=True)
    return tiles.reshape(-1, *tiles.shape[len(axes) :])


def two_step_exchange(array, groups, sequence, split_dim, concat_dim):
    size = lax.axis_size(groups[0]) * lax.axis_size(groups[1])
    tiles = in_blocks(array, split_dim, size)
    return joined_along(moved_by_axis(tiles, groups, sequence), concat_dim)


def normalize(entries, gain):
    wide = entries.astype(jnp.float32)
    factor = lax.rsqrt(jnp.mean(wide * wide, axis=-1, keepdims=True) + EPSILON)
    return wide * factor * gain.astype(jnp.float32)


def rotate(entries, positions):
    half = entries.shape[-1] // 2
    freqs = THETA ** (-jnp.arange(half, dtype=jnp.float32) / half)
    angle = positions.astype(jnp.float32)[:, None, None] * freqs[None, None, :]
    cosine = jnp.cos(angle)
    sine = jnp.sin(angle)
    first = entries[..., :half].astype(jnp.float32)
    second = entries[..., half:].astype(jnp.float32)
    turned = jnp.concatenate(
        [first * cosine - second * sine, first * sine + second * cosine], axis=-1
    )
    return turned.astype(jnp.bfloat16)


def rounded(entries):
    return lax.optimization_barrier(entries.astype(jnp.bfloat16)).astype(jnp.float32)


def attend(
    query_plain,
    query_rotary,
    latent_input,
    rotary_key,
    key_weight,
    value_weight,
    latent_gain,
    head_gain,
    out_weight,
):
    tokens = query_plain.shape[0]
    heads = key_weight.shape[1] // PLAIN_DIM
    offset = lax.axis_index(EP) * tokens
    positions = offset + jnp.arange(tokens, dtype=jnp.int32)
    last_position = offset + tokens - 1
    latent = normalize(latent_input, latent_gain).astype(jnp.bfloat16)
    key_rotated = rotate(rotary_key.reshape(tokens, 1, ROTARY_DIM), positions).reshape(
        tokens, ROTARY_DIM
    )
    query_rotated = rotate(query_rotary.reshape(tokens, heads, ROTARY_DIM), positions)
    queries = query_plain.reshape(tokens, heads, PLAIN_DIM)
    factor = (PLAIN_DIM + ROTARY_DIM) ** (-0.5)

    def reshape_given(piece):
        key_rows, value_rows, rotated_rows = piece
        count = key_rows.shape[0]
        return (
            key_rows.reshape(count, heads, PLAIN_DIM),
            value_rows.reshape(count, heads, VALUE_DIM),
            rotated_rows,
        )

    def add_keys(carry, unpacked, start):
        total, highest = carry
        keys, values, rotated_rows = unpacked
        count = keys.shape[0]
        scores = jnp.einsum("qhd,khd->qhk", queries, keys, preferred_element_type=jnp.float32)
        scores = scores + jnp.einsum(
            "qhr,kr->qhk", query_rotated, rotated_rows, preferred_element_type=jnp.float32
        )
        scores = scores * factor
        key_positions = start + jnp.arange(count, dtype=jnp.int32)
        allowed = (key_positions[None, :] <= positions[:, None])[:, None, :]
        masked = jnp.where(allowed, scores, -1e30)
        newest = jnp.maximum(highest, jnp.max(masked, axis=-1))
        weights = jnp.where(allowed, jnp.exp(masked - newest[..., None]), 0.0).astype(jnp.bfloat16)
        total = total * jnp.exp(highest - newest)[..., None] + jnp.einsum(
            "qhk,khd->qhd", weights, values, preferred_element_type=jnp.float32
        )
        return (total, newest)

    def make_fold(unpack):

        def guarded(carry, piece, start):

            def compute(state):
                return add_keys(state, unpack(piece), start)

            def keep(state):
                return state

            return lax.cond(start > last_position, keep, compute, carry)

        def fold(carry, piece, start):
            count = piece[0].shape[0]

            def step(index, inner):
                begin = index * key_span
                sliced = tuple(
                    (lax.dynamic_slice_in_dim(member, begin, key_span, 0) for member in piece)
                )
                return guarded(inner, sliced, begin)

            return lax.fori_loop(0, count // key_span, step, carry)

        return fold

    initial = (
        jnp.zeros((tokens, heads, VALUE_DIM), jnp.float32),
        jnp.full((tokens, heads), -1e30, jnp.float32),
    )
    own_keys = jnp.dot(latent, key_weight, preferred_element_type=jnp.float32).astype(jnp.bfloat16)
    own_values = jnp.dot(latent, value_weight, preferred_element_type=jnp.float32).astype(
        jnp.bfloat16
    )
    folded = make_fold(reshape_given)(
        initial, sent_together((own_keys, own_values, key_rotated), EP, 0, 1), jnp.int32(0)
    )
    context = folded[0]
    head_output = (
        normalize(context, head_gain.reshape(heads, VALUE_DIM))
        .astype(jnp.bfloat16)
        .reshape(tokens, heads * VALUE_DIM)
    )
    summed = sum_at_owner(
        rounded(jnp.dot(head_output, out_weight, preferred_element_type=jnp.float32)).astype(
            jnp.bfloat16
        ),
        "tp",
        0,
    )
    return summed.astype(jnp.bfloat16)


def experts(expert_input, expert_gain, routes, route_weight, gate_weight, up_weight, down_weight):
    tokens = expert_input.shape[0]
    features = expert_input.shape[1]
    count_ep = lax.axis_size(EP)
    capacity = min(tokens, max(2, (9 * tokens + 4 * count_ep - 1) // (4 * count_ep)))
    normed = normalize(expert_input, expert_gain).astype(jnp.bfloat16)
    chosen = routes.reshape(-1)
    onehot = (chosen[:, None] == jnp.arange(count_ep, dtype=jnp.int32)[None, :]).astype(jnp.int32)
    ranks = jnp.sum(jnp.cumsum(onehot, axis=0) * onehot, axis=1) - 1
    destination = chosen * capacity + ranks
    outgoing = (
        jnp.zeros((count_ep * capacity, features), jnp.bfloat16)
        .at[destination]
        .set(jnp.repeat(normed, TOP, axis=0))
    )
    gate_local = gate_weight[0]
    up_local = up_weight[0]
    down_local = down_weight[0]
    arrived = two_step_exchange(outgoing, ("ep_0", "ep_1"), (1, 0), 0, 0)
    piece = lax.all_gather(arrived, "tp", axis=0, tiled=True)
    gate = jnp.dot(piece, gate_local, preferred_element_type=jnp.float32)
    upward = jnp.dot(piece, up_local, preferred_element_type=jnp.float32)
    hidden = (jax.nn.silu(gate) * upward).astype(jnp.bfloat16)
    summed = sum_at_owner(
        rounded(jnp.dot(hidden, down_local, preferred_element_type=jnp.float32)).astype(
            jnp.bfloat16
        ),
        "tp",
        0,
    ).astype(jnp.bfloat16)
    returned = lax.all_to_all(summed, EP, split_axis=0, concat_axis=0, tiled=True)
    picked = returned[destination].astype(jnp.float32).reshape(tokens, TOP, features)
    combined = jnp.sum(picked * route_weight[:, :, None], axis=1)
    return combined.astype(jnp.bfloat16)


def body(
    query_plain,
    query_rotary,
    latent_input,
    rotary_key,
    key_weight,
    value_weight,
    latent_gain,
    head_gain,
    out_weight,
    expert_input,
    expert_gain,
    routes,
    route_weight,
    gate_weight,
    up_weight,
    down_weight,
):
    attended = attend(
        query_plain,
        query_rotary,
        latent_input,
        rotary_key,
        key_weight,
        value_weight,
        latent_gain,
        head_gain,
        out_weight,
    )
    expert_out = experts(
        expert_input, expert_gain, routes, route_weight, gate_weight, up_weight, down_weight
    )
    return (attended, expert_out)


def solution(mesh):
    finer = Mesh(
        mesh.devices.reshape(mesh.shape["grp"], 16, 2, mesh.shape["tp"]),
        ("grp", "ep_0", "ep_1", "tp"),
    )
    in_specs = (
        P(GRP_EP, "tp"),
        P(GRP_EP, "tp"),
        P(GRP_EP, None),
        P(GRP_EP, None),
        P(None, "tp"),
        P(None, "tp"),
        P(),
        P("tp"),
        P("tp", None),
        P(GRP_EP_TP, None),
        P(),
        P(GRP_EP_TP, None),
        P(GRP_EP_TP, None),
        P(EP, None, "tp"),
        P(EP, None, "tp"),
        P(EP, "tp", None),
    )
    out_specs = (P(GRP_EP_TP, None), P(GRP_EP_TP, None))
    return jax.shard_map(body, mesh=finer, in_specs=in_specs, out_specs=out_specs, check_vma=False)
```

profile of v0, /device:TPU:33, one launch (start us, length us, event | category | flops | bytes accessed | tf_op | source)
XLA Modules:
  0.0 412.7 jit_solution(7010274078072165320)
XLA Ops:
  7.2 0.0 copy-start
  7.2 0.1 all-gather.5.cloned.1.call-start
  7.3 0.8 copy.31
  8.1 0.1 eq.29
  8.2 0.1 eq.25
  8.4 0.7 broadcast_multiply_fusion
  9.1 0.6 reduce-window.6
  9.7 0.2 slice_reduce_fusion
  9.9 0.1 fusion.34
  10.0 0.1 copy.30
  10.1 0.1 mul.234
  10.2 0.7 convert_element_type.123
  10.9 1.2 fusion.19
  12.2 1.2 fusion.21
  13.4 0.6 broadcast_in_dim.62
  14.1 0.4 reshape.310
  14.5 3.2 scatter_custom_fusion
  17.7 1.6 reshape_reshape.6
  19.3 0.7 copy.34
  20.0 24.7 %all_to_all.32 = bf16[16,2,9,2048]{3,0,2,1:T(8,128)(2,1)S(1)} all-to-all(bf16[16,2,9,2048]{3,0,2,1:T(8,128)(2,1)S(1)} %copy.34), channel_id=1, replica_groups=mesh['grp'=2,'ep_0'=16,'ep_1'=2,'tp'=4] {'ep_1'}, dimensions={1} | all-to-all | bytes 2359296 | tf_op jit(solution)/shard_map/all_to_all | solution.py:50
  44.7 1.2 copy.35
  46.0 61.2 %all_to_all.33 = bf16[16,2,9,2048]{3,1,2,0:T(2,128)(2,1)S(1)} all-to-all(bf16[16,2,9,2048]{3,1,2,0:T(2,128)(2,1)S(1)} %copy.35), channel_id=1, replica_groups=mesh['grp'=2,'ep_0'=16,'ep_1'=2,'tp'=4] {'ep_0'}, dimensions={0} | all-to-all | bytes 2359296 | tf_op jit(solution)/shard_map/all_to_all | solution.py:50
  107.2 0.7 copy.36
  107.8 1.4 reshape_reshape.7
  109.2 0.1 all-gather.5.cloned.1.call-update
  109.3 0.2 all-gather.3.cloned.1.call-start
  109.6 0.1 fusion.24
  109.7 0.1 fusion.45
  109.9 0.3 convolution_convert_fusion.2
  110.2 0.3 convolution_convert_fusion.3
  110.5 0.7 pad_maximum_fusion
  111.1 0.1 all-gather.3.cloned.1.call-update
  111.2 53.7 %all-gather.5.cloned.1.call-done = bf16[1152,2048]{1,0:T(8,128)(2,1)} async-done(((bf16[288,2048]{1,0:T(8,128)(2,1)}), bf16[1152,2048]{1,0:T(8,128)(2,1)}) %all-gather.5.cloned.1.call-update) | async-done | bytes 4718608 | tf_op jit(solution)/shard_map/all_gather | solution.py:208
  164.9 8.1 %fusion.14 = f32[1152,896]{1,0:T(8,128)S(1)} fusion(bf16[1152,2048]{1,0:T(8,128)(2,1)} %all-gather.5.cloned.1.call-done, bf16[1,2048,896]{2,1,0:T(8,128)(2,1)} %param.33), kind=kOutput, calls=%fused_computation.25 | convolution fusion | flops 4227858432 | bytes 12517376 | tf_op jit(solution)/shard_map/dot_general | solution.py:209
  173.0 5.3 %fusion.16 = bf16[1152,896]{1,0:T(8,128)(2,1)S(1)} fusion(bf16[1152,2048]{1,0:T(8,128)(2,1)S(1)} %copy-done.6, bf16[1,2048,896]{2,1,0:T(8,128)(2,1)S(1)} %copy-done.7, f32[1152,896]{1,0:T(8,128)S(1)} %fusion.14), kind=kOutput, calls=%fused_computation.27 | convolution fusion | flops 4234051584 | bytes 14581760 | tf_op jit(solution)/shard_map/dot_general | solution.py:210
  178.4 6.8 %convolution_convert_fusion = bf16[1152,2048]{1,0:T(8,128)(2,1)} fusion(bf16[1152,896]{1,0:T(8,128)(2,1)S(1)} %fusion.16, bf16[1,896,2048]{2,1,0:T(8,128)(2,1)S(1)} %copy-done.8), kind=kOutput, calls=%fused_computation.21 | convolution fusion | flops 4230217728 | bytes 10452992 | tf_op jit(solution)/shard_map/dot_general | solution.py:213
  185.1 5.1 %all-to-all-start.3 = ((bf16[4,288,2048]{2,1,0:T(8,128)(2,1)}), bf16[4,288,2048]{2,1,0:T(8,128)(2,1)}, u32[]{:S(2)}, u32[]{:S(2)}) async-start(bf16[4,288,2048]{2,1,0:T(8,128)(2,1)} %bitcast.70), calls=%async_computation.3 | async-start | bytes 9437184 | tf_op jit(solution)/shard_map/all_to_all | solution.py:36
  190.3 0.1 copy.29
  190.4 0.1 reshape.296
  190.5 0.1 multiply_cosine_fusion
  190.7 57.7 %all-gather.3.cloned.1.call-done = bf16[8192,288]{0,1:T(8,128)(2,1)} async-done(((bf16[256,288]{0,1:T(8,128)(2,1)}), bf16[8192,288]{0,1:T(8,128)(2,1)}) %all-gather.3.cloned.1.call-update) | async-done | bytes 4718608 | tf_op jit(solution)/shard_map/all_gather | solution.py:25
  248.4 1.1 split.13
  249.5 3.9 fusion.47
  253.4 4.5 %while.16 = (s32[]{:T(128)}, f32[256,2,64]{0,2,1:T(8,128)S(1)}, f32[256,2]{0,1:T(2,128)S(1)}, s32[]{:T(128)}, bf16[8192,128]{0,1:T(8,128)(2,1)}, /*index=5*/bf16...) while((s32[]{:T(128)}, f32[256,2,64]{0,2,1:T(8,128)S(1)}, ...), condition=%wide.region_5.6_spmd.clone, body=%wide.region_1.5_spmd.clone.sunk | while | flops 343476992 | bytes 22022456 | solution.py:158
  253.4 4.3 %conditional.3 = ((f32[256,2,64]{0,2,1:T(8,128)S(1)}, f32[256,2]{0,1:T(2,128)S(1)})) conditional(s32[]{:T(128)} %convert_element_type.210, (s32[]{:T(128)}, s32[]{:T(128)}, bf16[8192,128]{0,1:T(8,128)(2,1)}, bf16[256,2,64]{0,2,1:T(8,128)(2,1)S(1)}, bf16[8192,32]{0,1:T(8,128)(2,1)S(1)}, /*index=5*/bf16[256,2,32]{0,2,1:T(8,128)(2,1)S(1)}, ...), branch_computations={%region_2.3_spmd, %region_4.4_spmd} | conditional | flops 343476992 | bytes 22021194 | solution.py:146
  253.5 1.1 constant_dynamic-slice_fusion
  254.6 0.8 fusion.48
  255.4 0.5 broadcast_compare_fusion
  255.8 1.1 fusion.46
  257.0 0.8 fusion.7
  258.0 0.1 multiply_convert_fusion
  258.1 1.4 convolution_convert_fusion.1
  259.5 3.7 all-to-all-start
  263.2 3.3 reduce_sum.74
  266.6 1.6 all_to_all.24
  268.2 9.7 %all-to-all-done = bf16[4,64,2048]{2,1,0:T(8,128)(2,1)S(1)} async-done(((bf16[4,64,2048]{2,1,0:T(8,128)(2,1)}), bf16[4,64,2048]{2,1,0:T(8,128)(2,1)S(1)}, u32[]{:S(2)}, u32[]{:S(2)}) %all-to-all-start) | async-done | bytes 1048608 | tf_op jit(solution)/shard_map/all_to_all | solution.py:36
  277.9 18.7 %all-to-all-start.4 = ((bf16[32,9,2048]{2,1,0:T(8,128)(2,1)}), bf16[32,9,2048]{2,1,0:T(8,128)(2,1)}, u32[]{:S(2)}, u32[]{:S(2)}) async-start(bf16[32,9,2048]{2,1,0:T(8,128)(2,1)} %all_to_all.24), calls=%async_computation.4 | async-start | bytes 4194304 | tf_op jit(solution)/shard_map/all_to_all | solution.py:219
  296.6 0.1 copy.37
  296.7 0.9 reduce_sum.71
  297.7 97.7 %all-to-all-done.4 = bf16[32,9,2048]{2,1,0:T(8,128)(2,1)} async-done(((bf16[32,9,2048]{2,1,0:T(8,128)(2,1)}), bf16[32,9,2048]{2,1,0:T(8,128)(2,1)}, u32[]{:S(2)}, u32[]{:S(2)}) %all-to-all-start.4) | async-done | bytes 1179680 | tf_op jit(solution)/shard_map/all_to_all | solution.py:219
  395.3 1.8 all_to_all.26
  397.2 2.3 gather_fusion
  399.5 2.4 reshape.297
  401.9 3.9 multiply_reduce_fusion
  (53 shorter events, 0.3 us)
Async XLA Ops:
  7.2 250.9 %copy-start = (bf16[128,2048]{1,0:T(8,128)(2,1)S(1)}, bf16[128,2048]{1,0:T(8,128)(2,1)}, u32[]{:S(2)}) copy-start(bf16[128,2048]{1,0:T(8,128)(2,1)} %param.28) | copy-start | bytes 1572868
  7.2 157.7 %all-gather.5.cloned.1.call-start = ((), (), s32[]{:S(2)}) async-start(), calls=%async_computation.6 | async-start | bytes 5898240 | tf_op jit(solution)/shard_map/all_gather | solution.py:208
  107.1 2.4 copy-start.11
  107.1 2.4 copy-start.1
  107.1 2.6 copy-start.4
  107.1 2.7 copy-start.9
  107.2 3.0 copy-start.10
  109.3 139.1 %all-gather.3.cloned.1.call-start = ((), (), s32[]{:S(2)}) async-start(), calls=%async_computation.5 | async-start | bytes 4866048 | tf_op jit(solution)/shard_map/all_gather | solution.py:25
  164.9 8.1 %copy-start.6 = (bf16[1152,2048]{1,0:T(8,128)(2,1)S(1)}, bf16[1152,2048]{1,0:T(8,128)(2,1)}, u32[]{:S(2)}) copy-start(bf16[1152,2048]{1,0:T(8,128)(2,1)} %all-gather.5.cloned.1.call-done) | copy-start | bytes 14155780
  164.9 8.1 %copy-start.7 = (bf16[1,2048,896]{2,1,0:T(8,128)(2,1)S(1)}, bf16[1,2048,896]{2,1,0:T(8,128)(2,1)}, u32[]{:S(2)}) copy-start(bf16[1,2048,896]{2,1,0:T(8,128)(2,1)} %param.34) | copy-start | bytes 11010052
  173.0 5.3 %copy-start.8 = (bf16[1,896,2048]{2,1,0:T(8,128)(2,1)S(1)}, bf16[1,896,2048]{2,1,0:T(8,128)(2,1)}, u32[]{:S(2)}) copy-start(bf16[1,896,2048]{2,1,0:T(8,128)(2,1)} %param.35) | copy-start | bytes 11010052
  185.1 5.2 %copy-start.2 = (bf16[256,128]{1,0:T(8,128)(2,1)S(1)}, bf16[256,128]{1,0:T(8,128)(2,1)}, u32[]{:S(2)}) copy-start(bf16[256,128]{1,0:T(8,128)(2,1)} %param.20) | copy-start | bytes 196612
  185.1 5.3 %copy-start.12 = (bf16[128]{0:T(256)(128)(2,1)S(1)}, bf16[128]{0:T(256)(128)(2,1)}, u32[]{:S(2)}) copy-start(bf16[128]{0:T(256)(128)(2,1)} %param.27) | copy-start | bytes 772
  185.1 5.5 %copy-start.3 = (bf16[256,64]{0,1:T(8,128)(2,1)S(1)}, bf16[256,64]{0,1:T(8,128)(2,1)}, u32[]{:S(2)}) copy-start(bf16[256,64]{0,1:T(8,128)(2,1)} %param.21) | copy-start | bytes 98308
  185.1 74.4 %all-to-all-start.3 = ((bf16[4,288,2048]{2,1,0:T(8,128)(2,1)}), bf16[4,288,2048]{2,1,0:T(8,128)(2,1)}, u32[]{:S(2)}, u32[]{:S(2)}) async-start(bf16[4,288,2048]{2,1,0:T(8,128)(2,1)} %bitcast.70), calls=%async_computation.3 | async-start | bytes 9437184 | tf_op jit(solution)/shard_map/all_to_all | solution.py:36
  259.5 18.3 %all-to-all-start = ((bf16[4,64,2048]{2,1,0:T(8,128)(2,1)}), bf16[4,64,2048]{2,1,0:T(8,128)(2,1)S(1)}, u32[]{:S(2)}, u32[]{:S(2)}) async-start(bf16[4,64,2048]{2,1,0:T(8,128)(2,1)} %bitcast.12), calls=%async_computation | async-start | bytes 2097152 | tf_op jit(solution)/shard_map/all_to_all | solution.py:36
  266.6 30.1 %copy-start.5 = (f32[128,2]{0,1:T(2,128)S(1)}, f32[128,2]{0,1:T(2,128)}, u32[]{:S(2)}) copy-start(f32[128,2]{0,1:T(2,128)} %param.32) | copy-start | bytes 3076
  277.9 117.5 %all-to-all-start.4 = ((bf16[32,9,2048]{2,1,0:T(8,128)(2,1)}), bf16[32,9,2048]{2,1,0:T(8,128)(2,1)}, u32[]{:S(2)}, u32[]{:S(2)}) async-start(bf16[32,9,2048]{2,1,0:T(8,128)(2,1)} %all_to_all.24), calls=%async_computation.4 | async-start | bytes 4194304 | tf_op jit(solution)/shard_map/all_to_all | solution.py:219
Sparse Core Ops, SparseCore 0:
  109.4 55.4 all-gather.4
  167.2 81.1 all-gather.2
where the time goes:
time: 414 us; the launch traced here: 413 us
  waiting for transfers between devices  219 us (53%)
  blocking collectives  85.9 us (21%)
  starting transfers between devices  27.9 us (7%)
  local copies, waits for them, and re-layouts  25.9 us (6%)
  matrix products  24.8 us (6%)
  other arithmetic  14.5 us (4%)
  between operations  14.5 us (4%)
    all_to_all x1, waiting for transfers between devices, experts(): lax.all_to_all(summed, EP, split_axis=0, concat_axis=0, tiled=True)  97.7 us
    all_to_all x2, blocking collectives, moved_by_axis(): lax.all_to_all(tiles, axes[k], split_axis=k, concat_axis=k, tiled=True)  85.9 us
    all_gather x1, waiting for transfers between devices, sent_together(): lax.all_gather(both, axis, axis=dim, tiled=True)  57.7 us
    all_gather x1, waiting for transfers between devices, experts(): piece = lax.all_gather(arrived, 'tp', axis=0, tiled=True)  53.7 us
    all_to_all x1, starting transfers between devices, experts(): lax.all_to_all(summed, EP, split_axis=0, concat_axis=0, tiled=True)  18.7 us
    all_to_all x2, waiting for transfers between devices, sum_at_owner(): tiles = lax.all_to_all(in_blocks(array, dim, size), axis, 0, 0, tiled=True)  9.7 us
    all_to_all x2, starting transfers between devices, sum_at_owner(): tiles = lax.all_to_all(in_blocks(array, dim, size), axis, 0, 0, tiled=True)  8.82 us
  transfers between devices with their start and end apart: 5, of which 4 were waited for; matrix products, arithmetic and copies ran while one was open for 9% of the time, Pallas kernels for 0%

commit v1 on v0

--- a/solution.py
+++ b/solution.py
@@ -205,7 +205,15 @@
     up_local = up_weight[0]
     down_local = down_weight[0]
     arrived = two_step_exchange(outgoing, ("ep_0", "ep_1"), (1, 0), 0, 0)
-    piece = lax.all_gather(arrived, "tp", axis=0, tiled=True)
+    count_2, place, width = (lax.axis_size("tp"), lax.axis_index("tp"), arrived.shape[0])
+    right = [(i, (i + 1) % count_2) for i in range(count_2)]
+    piece = jnp.zeros((*arrived.shape[:0], count_2 * width, *arrived.shape[0 + 1 :]), arrived.dtype)
+    current = arrived
+    for step_2 in range(count_2):
+        holder = (place - step_2) % count_2
+        piece = lax.dynamic_update_slice_in_dim(piece, current, holder * width, axis=0)
+        if step_2 < count_2 - 1:
+            current = lax.ppermute(current, "tp", right)
     gate = jnp.dot(piece, gate_local, preferred_element_type=jnp.float32)
     upward = jnp.dot(piece, up_local, preferred_element_type=jnp.float32)
     hidden = (jax.nn.silu(gate) * upward).astype(jnp.bfloat16)

time: 414 us -> 420 us (1.014)
  blocking collectives: 85.9 us -> 24.9 us
  waiting for transfers between devices: 219 us -> 261 us
  starting transfers between devices: 27.9 us -> 50.2 us
  local copies, waits for them, and re-layouts: 25.9 us -> 32.1 us
    ppermute x0 -> x3, waiting for transfers between devices: none -> 68.8 us  [experts(): current = lax.ppermute(current, 'tp', right)]
    all_to_all x2 -> x1, blocking collectives: 85.9 us -> 24.9 us  [moved_by_axis(): lax.all_to_all(tiles, axes[k], split_axis=k, concat_axis=k, tiled=True)]
    all_gather x1, waiting for transfers between devices: 57.7 us -> 0.02 us  [sent_together(): lax.all_gather(both, axis, axis=dim, tiled=True)]
    all_to_all x0 -> x1, waiting for transfers between devices: none -> 54.4 us  [moved_by_axis(): lax.all_to_all(tiles, axes[k], split_axis=k, concat_axis=k, tiled=True)]
    all_gather x1 -> x0, waiting for transfers between devices: 53.7 us -> none  [experts(): piece = lax.all_gather(arrived, 'tp', axis=0, tiled=True)]
    all_to_all x2, waiting for transfers between devices: 9.7 us -> 39.8 us  [sum_at_owner(): tiles = lax.all_to_all(in_blocks(array, dim, size), axis, 0, 0, tiled=True)]
    all_to_all x1, starting transfers between devices: 18.7 us -> 35 us  [experts(): lax.all_to_all(summed, EP, split_axis=0, concat_axis=0, tiled=True)]
    all_to_all x0 -> x1, starting transfers between devices: none -> 4.79 us  [moved_by_axis(): lax.all_to_all(tiles, axes[k], split_axis=k, concat_axis=k, tiled=True)]
  transfers between devices with their start and end apart: 5 -> 8, of which waited for: 4 -> 7; matrix products, arithmetic and copies ran while one was open for 9% -> 10% of each run, Pallas kernels for 0% -> 0%
where the time goes in v1:
time: 420 us; the launch traced here: 419 us
  waiting for transfers between devices  261 us (62%)
  starting transfers between devices  50.2 us (12%)
  local copies, waits for them, and re-layouts  32.1 us (8%)
  blocking collectives  24.9 us (6%)
  matrix products  21.8 us (5%)
  between operations  14.6 us (3%)
  other arithmetic  14.5 us (3%)
    all_to_all x1, waiting for transfers between devices, experts(): lax.all_to_all(summed, EP, split_axis=0, concat_axis=0, tiled=True)  97.7 us
    ppermute x3, waiting for transfers between devices, experts(): current = lax.ppermute(current, 'tp', right)  68.8 us
    all_to_all x1, waiting for transfers between devices, moved_by_axis(): lax.all_to_all(tiles, axes[k], split_axis=k, concat_axis=k, tiled=True)  54.4 us
    all_to_all x2, waiting for transfers between devices, sum_at_owner(): tiles = lax.all_to_all(in_blocks(array, dim, size), axis, 0, 0, tiled=True)  39.8 us
    all_to_all x1, starting transfers between devices, experts(): lax.all_to_all(summed, EP, split_axis=0, concat_axis=0, tiled=True)  35 us
    all_to_all x1, blocking collectives, moved_by_axis(): lax.all_to_all(tiles, axes[k], split_axis=k, concat_axis=k, tiled=True)  24.9 us
    all_to_all x2, starting transfers between devices, sum_at_owner(): tiles = lax.all_to_all(in_blocks(array, dim, size), axis, 0, 0, tiled=True)  9.01 us
  transfers between devices with their start and end apart: 8, of which 7 were waited for; matrix products, arithmetic and copies ran while one was open for 10% of the time, Pallas kernels for 0%

profile of v1, /device:TPU:33, one launch (start us, length us, event | category | flops | bytes accessed | tf_op | source)
XLA Modules:
  0.0 419.1 jit_solution(11127622951917714148)
XLA Ops:
  7.2 0.8 copy.31
  8.0 0.1 eq.34
  8.2 0.1 eq.30
  8.3 0.7 broadcast_multiply_fusion
  9.0 0.6 reduce-window.6
  9.6 0.2 slice_reduce_fusion
  9.9 0.1 copy.30
  10.0 0.1 mul.246
  10.2 0.7 convert_element_type.123
  10.9 1.2 fusion.19
  12.1 1.2 fusion.21
  13.4 0.6 broadcast_in_dim.66
  14.0 0.4 reshape.310
  14.5 3.2 scatter_custom_fusion
  17.7 1.6 reshape_reshape.6
  19.2 0.7 copy.34
  20.0 24.9 %all_to_all.32 = bf16[16,2,9,2048]{3,0,2,1:T(8,128)(2,1)S(1)} all-to-all(bf16[16,2,9,2048]{3,0,2,1:T(8,128)(2,1)S(1)} %copy.34), channel_id=1, replica_groups=mesh['grp'=2,'ep_0'=16,'ep_1'=2,'tp'=4] {'ep_1'}, dimensions={1} | all-to-all | bytes 2359296 | tf_op jit(solution)/shard_map/all_to_all | solution.py:50
  44.9 2.2 copy.35
  47.1 4.8 %all-to-all-start.2 = ((bf16[16,2,9,2048]{3,1,2,0:T(2,128)(2,1)}), bf16[16,2,9,2048]{3,1,2,0:T(2,128)(2,1)}, u32[]{:S(2)}, u32[]{:S(2)}) async-start(bf16[16,2,9,2048]{3,1,2,0:T(2,128)(2,1)} %copy.35), calls=%async_computation.2 | async-start | bytes 2359296 | tf_op jit(solution)/shard_map/all_to_all | solution.py:50
  52.1 0.1 fusion.24
  52.2 0.1 fusion.45
  52.4 0.3 convolution_convert_fusion.2
  52.6 0.3 convolution_convert_fusion.3
  52.9 0.7 pad_maximum_fusion
  53.7 54.4 %all-to-all-done.2 = bf16[16,2,9,2048]{3,1,2,0:T(2,128)(2,1)} async-done(((bf16[16,2,9,2048]{3,1,2,0:T(2,128)(2,1)}), bf16[16,2,9,2048]{3,1,2,0:T(2,128)(2,1)}, u32[]{:S(2)}, u32[]{:S(2)}) %all-to-all-start.2) | async-done | bytes 1179680 | tf_op jit(solution)/shard_map/all_to_all | solution.py:50
  108.1 1.9 copy.36
  110.0 1.4 reshape_reshape.7
  111.4 1.3 collective-permute-start
  112.7 22.4 %collective-permute-done = bf16[288,2048]{1,0:T(8,128)(2,1)S(1)} collective-permute-done((bf16[288,2048]{1,0:T(8,128)(2,1)}, bf16[288,2048]{1,0:T(8,128)(2,1)S(1)}, u32[]{:S(2)}, u32[]{:S(2)}) %collective-permute-start) | collective-permute-done | bytes 1179680 | tf_op jit(solution)/shard_map/ppermute | solution.py:216
  135.1 24.5 %collective-permute-done.1 = bf16[288,2048]{1,0:T(8,128)(2,1)} collective-permute-done((bf16[288,2048]{1,0:T(8,128)(2,1)S(1)}, bf16[288,2048]{1,0:T(8,128)(2,1)}, u32[]{:S(2)}, u32[]{:S(2)}) %collective-permute-start.1) | collective-permute-done | bytes 1179680 | tf_op jit(solution)/shard_map/ppermute | solution.py:216
  159.6 0.6 broadcast_in_dim.64
  160.2 0.1 constant_dynamic-update-slice_fusion.3
  160.4 0.1 constant_dynamic-update-slice_fusion.2
  160.5 1.6 constant_dynamic-update-slice_fusion.1
  162.1 22.0 %collective-permute-done.2 = bf16[288,2048]{1,0:T(8,128)(2,1)} collective-permute-done((bf16[288,2048]{1,0:T(8,128)(2,1)}, bf16[288,2048]{1,0:T(8,128)(2,1)}, u32[]{:S(2)}, u32[]{:S(2)}) %collective-permute-start.2) | collective-permute-done | bytes 1179680 | tf_op jit(solution)/shard_map/ppermute | solution.py:216
  184.1 1.4 constant_dynamic-update-slice_fusion
  185.5 5.1 %fusion.17 = f32[1152,896]{1,0:T(8,128)S(1)} fusion(bf16[1152,2048]{1,0:T(8,128)(2,1)S(1)} %constant_dynamic-update-slice_fusion, bf16[1,2048,896]{2,1,0:T(8,128)(2,1)S(1)} %copy-done.7), kind=kOutput, calls=%fused_computation.26 | convolution fusion | flops 4227858432 | bytes 12517376 | tf_op jit(solution)/shard_map/dot_general | solution.py:217
  190.6 5.3 %multiply_convert_fusion = bf16[1152,896]{1,0:T(8,128)(2,1)S(1)} fusion(f32[1152,896]{1,0:T(8,128)S(1)} %fusion.17, bf16[1152,2048]{1,0:T(8,128)(2,1)S(1)} %constant_dynamic-update-slice_fusion, bf16[1,2048,896]{2,1,0:T(8,128)(2,1)S(1)} %copy-done.8), kind=kOutput, calls=%fused_computation.22 | convolution fusion | flops 4234051584 | bytes 14581760 | tf_op jit(solution)/shard_map/dot_general | solution.py:218
  195.9 6.7 %convolution_convert_fusion = bf16[1152,2048]{1,0:T(8,128)(2,1)} fusion(bf16[1152,896]{1,0:T(8,128)(2,1)S(1)} %multiply_convert_fusion, bf16[1,896,2048]{2,1,0:T(8,128)(2,1)S(1)} %copy-done.9), kind=kOutput, calls=%fused_computation.21 | convolution fusion | flops 4230217728 | bytes 10452992 | tf_op jit(solution)/shard_map/dot_general | solution.py:221
  202.7 5.2 %all-to-all-start.3 = ((bf16[4,288,2048]{2,1,0:T(8,128)(2,1)}), bf16[4,288,2048]{2,1,0:T(8,128)(2,1)}, u32[]{:S(2)}, u32[]{:S(2)}) async-start(bf16[4,288,2048]{2,1,0:T(8,128)(2,1)} %bitcast.70), calls=%async_computation.3 | async-start | bytes 9437184 | tf_op jit(solution)/shard_map/all_to_all | solution.py:36
  208.1 0.1 multiply_cosine_fusion
  208.3 1.1 split.13
  209.4 3.9 fusion.47
  213.3 4.5 %while.16 = (s32[]{:T(128)}, f32[256,2,64]{0,2,1:T(8,128)S(1)}, f32[256,2]{0,1:T(2,128)S(1)}, s32[]{:T(128)}, bf16[8192,128]{0,1:T(8,128)(2,1)}, /*index=5*/bf16...) while((s32[]{:T(128)}, f32[256,2,64]{0,2,1:T(8,128)S(1)}, ...), condition=%wide.region_5.6_spmd.clone, body=%wide.region_1.5_spmd.clone.sunk | while | flops 343476992 | bytes 22022456 | solution.py:158
  213.4 4.3 %conditional.3 = ((f32[256,2,64]{0,2,1:T(8,128)S(1)}, f32[256,2]{0,1:T(2,128)S(1)})) conditional(s32[]{:T(128)} %convert_element_type.210, (s32[]{:T(128)}, s32[]{:T(128)}, bf16[8192,128]{0,1:T(8,128)(2,1)}, bf16[256,2,64]{0,2,1:T(8,128)(2,1)S(1)}, bf16[8192,32]{0,1:T(8,128)(2,1)S(1)}, /*index=5*/bf16[256,2,32]{0,2,1:T(8,128)(2,1)S(1)}, ...), branch_computations={%region_2.3_spmd, %region_4.4_spmd} | conditional | flops 343476992 | bytes 22021194 | solution.py:146
  213.4 1.1 constant_dynamic-slice_fusion
  214.5 0.8 fusion.48
  215.3 0.5 broadcast_compare_fusion
  215.8 1.1 fusion.46
  216.9 0.8 fusion.7
  218.0 1.4 convolution_convert_fusion.1
  219.5 34.9 %all-to-all-done.3 = bf16[4,288,2048]{2,1,0:T(8,128)(2,1)} async-done(((bf16[4,288,2048]{2,1,0:T(8,128)(2,1)}), bf16[4,288,2048]{2,1,0:T(8,128)(2,1)}, u32[]{:S(2)}, u32[]{:S(2)}) %all-to-all-start.3) | async-done | bytes 4718624 | tf_op jit(solution)/shard_map/all_to_all | solution.py:36
  254.3 3.8 all-to-all-start
  258.2 3.3 reduce_sum.74
  261.5 1.6 all_to_all.24
  263.1 5.0 %all-to-all-done = bf16[4,64,2048]{2,1,0:T(8,128)(2,1)S(1)} async-done(((bf16[4,64,2048]{2,1,0:T(8,128)(2,1)}), bf16[4,64,2048]{2,1,0:T(8,128)(2,1)S(1)}, u32[]{:S(2)}, u32[]{:S(2)}) %all-to-all-start) | async-done | bytes 1048608 | tf_op jit(solution)/shard_map/all_to_all | solution.py:36
  268.1 35.0 %all-to-all-start.4 = ((bf16[32,9,2048]{2,1,0:T(8,128)(2,1)}), bf16[32,9,2048]{2,1,0:T(8,128)(2,1)}, u32[]{:S(2)}, u32[]{:S(2)}) async-start(bf16[32,9,2048]{2,1,0:T(8,128)(2,1)} %all_to_all.24), calls=%async_computation.4 | async-start | bytes 4194304 | tf_op jit(solution)/shard_map/all_to_all | solution.py:227
  303.1 0.1 copy.37
  303.2 0.9 reduce_sum.71
  304.2 97.7 %all-to-all-done.4 = bf16[32,9,2048]{2,1,0:T(8,128)(2,1)} async-done(((bf16[32,9,2048]{2,1,0:T(8,128)(2,1)}), bf16[32,9,2048]{2,1,0:T(8,128)(2,1)}, u32[]{:S(2)}, u32[]{:S(2)}) %all-to-all-start.4) | async-done | bytes 1179680 | tf_op jit(solution)/shard_map/all_to_all | solution.py:227
  401.8 1.8 all_to_all.26
  403.7 2.3 gather_fusion
  406.0 2.4 reshape.297
  408.4 3.9 multiply_reduce_fusion
  (64 shorter events, 0.8 us)
Async XLA Ops:
  7.2 210.9 %copy-start = (bf16[128,2048]{1,0:T(8,128)(2,1)S(1)}, bf16[128,2048]{1,0:T(8,128)(2,1)}, u32[]{:S(2)}) copy-start(bf16[128,2048]{1,0:T(8,128)(2,1)} %param.28) | copy-start | bytes 1572868
  20.0 32.0 %copy-start.12 = (bf16[256]{0:T(256)(128)(2,1)S(1)}, bf16[256]{0:T(256)(128)(2,1)}, u32[]{:S(2)}) copy-start(bf16[256]{0:T(256)(128)(2,1)} %param.26) | copy-start | bytes 1540
  20.0 32.1 %copy-start.2 = (bf16[256,256]{1,0:T(8,128)(2,1)S(1)}, bf16[256,256]{1,0:T(8,128)(2,1)}, u32[]{:S(2)}) copy-start(bf16[256,256]{1,0:T(8,128)(2,1)} %param.22) | copy-start | bytes 393220
  20.0 32.2 %copy-start.5 = (bf16[256,32]{0,1:T(8,128)(2,1)S(1)}, bf16[256,32]{0,1:T(8,128)(2,1)}, u32[]{:S(2)}) copy-start(bf16[256,32]{0,1:T(8,128)(2,1)} %param.23) | copy-start | bytes 49156
  20.0 32.4 %copy-start.10 = (bf16[256,128]{1,0:T(8,128)(2,1)S(1)}, bf16[256,128]{1,0:T(8,128)(2,1)}, u32[]{:S(2)}) copy-start(bf16[256,128]{1,0:T(8,128)(2,1)} %param.25) | copy-start | bytes 196612
  20.0 32.6 %copy-start.11 = (bf16[256,128]{1,0:T(8,128)(2,1)S(1)}, bf16[256,128]{1,0:T(8,128)(2,1)}, u32[]{:S(2)}) copy-start(bf16[256,128]{1,0:T(8,128)(2,1)} %param.24) | copy-start | bytes 196612
  47.1 60.9 %all-to-all-start.2 = ((bf16[16,2,9,2048]{3,1,2,0:T(2,128)(2,1)}), bf16[16,2,9,2048]{3,1,2,0:T(2,128)(2,1)}, u32[]{:S(2)}, u32[]{:S(2)}) async-start(bf16[16,2,9,2048]{3,1,2,0:T(2,128)(2,1)} %copy.35), calls=%async_computation.2 | async-start | bytes 2359296 | tf_op jit(solution)/shard_map/all_to_all | solution.py:50
  51.9 156.4 %all-gather.2.cloned.1.call-start = ((), (), s32[]{:S(2)}) async-start(), calls=%async_computation.5 | async-start | bytes 4866048 | tf_op jit(solution)/shard_map/all_gather | solution.py:25
  111.4 48.8 %copy-start.1 = (bf16[288,2048]{1,0:T(8,128)(2,1)S(1)}, bf16[288,2048]{1,0:T(8,128)(2,1)}, u32[]{:S(2)}) copy-start(bf16[288,2048]{1,0:T(8,128)(2,1)} %reshape_reshape.7) | copy-start | bytes 3538948
  111.4 23.7 %collective-permute-start = (bf16[288,2048]{1,0:T(8,128)(2,1)}, bf16[288,2048]{1,0:T(8,128)(2,1)S(1)}, u32[]{:S(2)}, u32[]{:S(2)}) collective-permute-start(bf16[288,2048]{1,0:T(8,128)(2,1)} %reshape_reshape.7), channel_id=1, source_target_pairs={{0,1},{1,2},{2,3},{3,0},{4,5},{5,6},{6,7},{7,4},{8,9},{9,10},{10,1... | collective-permute-start | bytes 3538952 | tf_op jit(solution)/shard_map/ppermute | solution.py:216
  135.1 24.5 %collective-permute-start.1 = (bf16[288,2048]{1,0:T(8,128)(2,1)S(1)}, bf16[288,2048]{1,0:T(8,128)(2,1)}, u32[]{:S(2)}, u32[]{:S(2)}) collective-permute-start(bf16[288,2048]{1,0:T(8,128)(2,1)S(1)} %collective-permute-done), channel_id=1, source_target_pairs={{0,1},{1,2},{2,3},{3,0},{4,5},{5,6},{6,7},{7,4},{8,9},{9,10},{10,1... | collective-permute-start | bytes 3538952 | tf_op jit(solution)/shard_map/ppermute | solution.py:216
  159.6 24.4 %collective-permute-start.2 = (bf16[288,2048]{1,0:T(8,128)(2,1)}, bf16[288,2048]{1,0:T(8,128)(2,1)}, u32[]{:S(2)}, u32[]{:S(2)}) collective-permute-start(bf16[288,2048]{1,0:T(8,128)(2,1)} %collective-permute-done.1), channel_id=1, source_target_pairs={{0,1},{1,2},{2,3},{3,0},{4,5},{5,6},{6,7},{7,4},{8,9},{9,10},{10,1... | collective-permute-start | bytes 3538952 | tf_op jit(solution)/shard_map/ppermute | solution.py:216
  160.4 25.1 %copy-start.7 = (bf16[1,2048,896]{2,1,0:T(8,128)(2,1)S(1)}, bf16[1,2048,896]{2,1,0:T(8,128)(2,1)}, u32[]{:S(2)}) copy-start(bf16[1,2048,896]{2,1,0:T(8,128)(2,1)} %param.33) | copy-start | bytes 11010052
  185.5 5.1 %copy-start.8 = (bf16[1,2048,896]{2,1,0:T(8,128)(2,1)S(1)}, bf16[1,2048,896]{2,1,0:T(8,128)(2,1)}, u32[]{:S(2)}) copy-start(bf16[1,2048,896]{2,1,0:T(8,128)(2,1)} %param.34) | copy-start | bytes 11010052
  190.6 5.3 %copy-start.9 = (bf16[1,896,2048]{2,1,0:T(8,128)(2,1)S(1)}, bf16[1,896,2048]{2,1,0:T(8,128)(2,1)}, u32[]{:S(2)}) copy-start(bf16[1,896,2048]{2,1,0:T(8,128)(2,1)} %param.35) | copy-start | bytes 11010052
  202.7 5.2 %copy-start.3 = (bf16[256,128]{1,0:T(8,128)(2,1)S(1)}, bf16[256,128]{1,0:T(8,128)(2,1)}, u32[]{:S(2)}) copy-start(bf16[256,128]{1,0:T(8,128)(2,1)} %param.20) | copy-start | bytes 196612
  202.7 5.3 %copy-start.13 = (bf16[128]{0:T(256)(128)(2,1)S(1)}, bf16[128]{0:T(256)(128)(2,1)}, u32[]{:S(2)}) copy-start(bf16[128]{0:T(256)(128)(2,1)} %param.27) | copy-start | bytes 772
  202.7 5.6 %copy-start.4 = (bf16[256,64]{0,1:T(8,128)(2,1)S(1)}, bf16[256,64]{0,1:T(8,128)(2,1)}, u32[]{:S(2)}) copy-start(bf16[256,64]{0,1:T(8,128)(2,1)} %param.21) | copy-start | bytes 98308
  202.7 51.6 %all-to-all-start.3 = ((bf16[4,288,2048]{2,1,0:T(8,128)(2,1)}), bf16[4,288,2048]{2,1,0:T(8,128)(2,1)}, u32[]{:S(2)}, u32[]{:S(2)}) async-start(bf16[4,288,2048]{2,1,0:T(8,128)(2,1)} %bitcast.70), calls=%async_computation.3 | async-start | bytes 9437184 | tf_op jit(solution)/shard_map/all_to_all | solution.py:36
  254.3 13.7 %all-to-all-start = ((bf16[4,64,2048]{2,1,0:T(8,128)(2,1)}), bf16[4,64,2048]{2,1,0:T(8,128)(2,1)S(1)}, u32[]{:S(2)}, u32[]{:S(2)}) async-start(bf16[4,64,2048]{2,1,0:T(8,128)(2,1)} %bitcast.12), calls=%async_computation | async-start | bytes 2097152 | tf_op jit(solution)/shard_map/all_to_all | solution.py:36
  261.5 41.6 %copy-start.6 = (f32[128,2]{0,1:T(2,128)S(1)}, f32[128,2]{0,1:T(2,128)}, u32[]{:S(2)}) copy-start(f32[128,2]{0,1:T(2,128)} %param.32) | copy-start | bytes 3076
  268.1 133.7 %all-to-all-start.4 = ((bf16[32,9,2048]{2,1,0:T(8,128)(2,1)}), bf16[32,9,2048]{2,1,0:T(8,128)(2,1)}, u32[]{:S(2)}, u32[]{:S(2)}) async-start(bf16[32,9,2048]{2,1,0:T(8,128)(2,1)} %all_to_all.24), calls=%async_computation.4 | async-start | bytes 4194304 | tf_op jit(solution)/shard_map/all_to_all | solution.py:227
Sparse Core Ops, SparseCore 0:
  55.1 107.7 all-gather.1
